TPU v7x, 256 devices: a whole 4x4x8 slice. The times are simulated.
256 devices in a mesh: ra: 32 (over z, y), cb: 8 (over x, core).
Axes of the slice: x: 4, y: 4, z: 8, core: 2. Of those that a mesh axis runs over, the one named last changes fastest.
Arguments:
- stream: bfloat16 [64, 1024], P(None, 'ra'), may hold values from -24 to 24, as said below
- gain_first: float32 [1024], P('ra'), may hold values from 0.5 to 1.5
- up_first: float32 [1024, 4096], P('ra', 'cb'), may hold values from -0.1875 to 0.1875
- down_first: float32 [4096, 1024], P('cb', 'ra'), may hold values from -0.09375 to 0.09375
- gain_second: float32 [1024], P('ra'), may hold values from 0.5 to 1.5
- up_second: float32 [1024, 4096], P('ra', 'cb'), may hold values from -0.1875 to 0.1875
- down_second: float32 [4096, 1024], P('cb', 'ra'), may hold values from -0.09375 to 0.09375
Outputs:
- read: bfloat16 [64, 1024], P(None, 'ra')
Inputs may be any that keep to these rules, and one draw needn't show every extreme that they name: stream is of order one, and in each token one aligned block of 32 features is four times larger than the rest.
All inputs are finite; a program needn't handle non-finite values.
Results may differ from a plain program's by a relative error of at most 0.025.
Values may be sent and summed in bfloat16 or wider, within the bound.
A program may use at most 64 MiB of HBM per device.

v0:
```python
import functools

import jax
import jax.numpy as jnp
from jax import lax
from jax.experimental import pallas as pl
from jax.experimental.pallas import tpu as pltpu
from jax.sharding import PartitionSpec as P

EPS = 1e-06
RESIDUAL = 0.25
LANES = 128
ROWS = 8
MESH = pl.DeviceIdType.MESH
F32 = jnp.float32
BF16 = jnp.bfloat16


def kernel(
    n, m, width,
    stream_hbm, gain1_hbm, up1_hbm, down1_hbm, gain2_hbm, up2_hbm, down2_hbm,
    out_ref,
    stream_v, gain_v, up_v, up_b, down_v, down_b,
    part_out, part_in, sq_out, sq_in, act, branch_in,
    load_sem, part_ss, part_rs, sq_ss, sq_rs, act_ss, act_rs, br_ss, br_rs,
):
    ra = lax.axis_index("ra")
    cb = lax.axis_index("cb")
    tokens = stream_v.shape[0]
    block = part_out.shape[-1]

    pair = 2 if n % 2 == 0 else 1
    half = lax.div(2 * ra, n)
    own_group = half * lax.div(ra, pair) + (1 - half) * (n // pair - 1 - lax.div(ra, pair))
    own_place = pair * own_group

    def ra_peer(step):
        place = step - 1
        place = place + lax.div(place - own_place + n, n)
        group = lax.div(place, pair)
        group = half * group + (1 - half) * (n // pair - 1 - group)
        return pair * group + lax.rem(ra + place, pair)

    def cb_peer(step):
        return lax.rem(cb + step, m)

    loads = [
        pltpu.make_async_copy(src, dst, load_sem.at[i])
        for i, (src, dst) in enumerate((
            (stream_hbm, stream_v),
            (gain1_hbm, gain_v.at[0]),
            (up1_hbm, up_v.at[0]),
            (down1_hbm, down_v.at[0]),
            (gain2_hbm, gain_v.at[1]),
            (up2_hbm, up_v.at[1]),
            (down2_hbm, down_v.at[1]),
        ))
    ]
    barrier = pltpu.get_barrier_semaphore()
    for step in range(1, n):
        pl.semaphore_signal(barrier, inc=1, device_id={"ra": ra_peer(step)}, device_id_type=MESH)
    for step in range(1, m):
        pl.semaphore_signal(barrier, inc=1, device_id={"cb": cb_peer(step)}, device_id_type=MESH)
    for load in loads:
        load.start()

    def to_ra(src, dst, send, recv, peer):
        return pltpu.make_async_remote_copy(
            src_ref=src, dst_ref=dst, send_sem=send, recv_sem=recv,
            device_id={"ra": peer}, device_id_type=MESH,
        )

    def to_cb(src, dst, send, recv, peer):
        return pltpu.make_async_remote_copy(
            src_ref=src, dst_ref=dst, send_sem=send, recv_sem=recv,
            device_id={"cb": peer}, device_id_type=MESH,
        )

    sends = []
    for load in loads[:2]:
        load.wait()
    floated = stream_v[...].astype(F32)
    result = None
    for layer in range(2):
        scaled = (floated * gain_v[layer]).astype(BF16)
        if layer == 0:
            loads[2].wait()
        up = up_v[layer].astype(BF16) if layer == 0 else up_b[...]
        partial = jnp.dot(scaled, up, preferred_element_type=F32)
        for j in range(n):
            part_out[layer, j] = partial[:, j * block:(j + 1) * block].astype(BF16)
        if layer == 0:
            pl.semaphore_wait(barrier, n + m - 2)
        copies = []
        for step in range(1, n):
            peer = ra_peer(step)
            copies.append(to_ra(
                part_out.at[layer, peer], part_in.at[layer, ra],
                part_ss.at[layer, peer], part_rs.at[layer, ra], peer))
        for copy in copies:
            copy.start()
        sends += copies
        own = jnp.sum(floated * floated, axis=1, keepdims=True)
        sq_out[layer] = jnp.broadcast_to(own, (tokens, LANES)).T[:ROWS]
        copies = []
        for step in range(1, n):
            peer = ra_peer(step)
            copies.append(to_ra(
                sq_out.at[layer], sq_in.at[layer, ra],
                sq_ss.at[layer, peer], sq_rs.at[layer, ra], peer))
        for copy in copies:
            copy.start()
        sends += copies

        loads[3 + 3 * layer].wait()
        for j in range(n):
            down_b[layer, j] = down_v[layer, j * block:(j + 1) * block, :].astype(BF16)

        preact = part_out[layer, ra].astype(F32)
        for step in range(1, n):
            peer = ra_peer(step)
            to_ra(part_out.at[layer, peer], part_in.at[layer, peer],
                  part_ss.at[layer, peer], part_rs.at[layer, peer], peer).wait_recv()
            preact += part_in[layer, peer].astype(F32)
        positive = jnp.maximum(preact, 0.0)
        act[layer, ra] = (positive * positive).astype(BF16)

        copies = []
        for step in range(1, n):
            peer = ra_peer(step)
            copies.append(to_ra(
                act.at[layer, ra], act.at[layer, ra],
                act_ss.at[layer, peer], act_rs.at[layer, ra], peer))
        for copy in copies:
            copy.start()
        sends += copies

        if layer == 0:
            loads[5].wait()
            up_b[...] = up_v[1].astype(BF16)

        squares = sq_out[layer]
        for step in range(1, n):
            peer = ra_peer(step)
            to_ra(sq_out.at[layer], sq_in.at[layer, peer],
                  sq_ss.at[layer, peer], sq_rs.at[layer, peer], peer).wait_recv()
            squares += sq_in[layer, peer]
        factor = 1.0 / (squares / width + EPS)
        scale = jnp.broadcast_to(factor[:1], (LANES, tokens)).T[:, :1]

        total = jnp.dot(act[layer, ra], down_b[layer, ra], preferred_element_type=F32)
        for step in range(1, n):
            peer = ra_peer(step)
            to_ra(act.at[layer, peer], act.at[layer, peer],
                  act_ss.at[layer, peer], act_rs.at[layer, peer], peer).wait_recv()
            total += jnp.dot(act[layer, peer], down_b[layer, peer], preferred_element_type=F32)

        branch_in[layer, cb] = (total * scale).astype(BF16)
        copies = []
        for step in range(1, m):
            peer = cb_peer(step)
            copies.append(to_cb(
                branch_in.at[layer, cb], branch_in.at[layer, cb],
                br_ss.at[layer, peer], br_rs.at[layer, cb], peer))
        for copy in copies:
            copy.start()
        sends += copies
        if layer == 0:
            loads[4].wait()
        for step in range(1, m):
            peer = cb_peer(step)
            to_cb(branch_in.at[layer, peer], branch_in.at[layer, peer],
                  br_ss.at[layer, peer], br_rs.at[layer, peer], peer).wait_recv()
        branch = branch_in[layer, 0].astype(F32)
        for j in range(1, m):
            branch += branch_in[layer, j].astype(F32)
        result = (RESIDUAL * floated + branch).astype(BF16)
        floated = result.astype(F32)
    out_ref[...] = result
    for copy in sends:
        copy.wait_send()


def local(n, m, stream, gain_first, up_first, down_first, gain_second, up_second, down_second):
    tokens, cols = stream.shape
    hidden = up_first.shape[1]
    block = hidden // n
    dma = pltpu.SemaphoreType.DMA
    return pl.pallas_call(
        functools.partial(kernel, n, m, cols * n),
        out_shape=jax.ShapeDtypeStruct((tokens, cols), BF16),
        in_specs=[pl.BlockSpec(memory_space=pl.ANY)] * 7,
        out_specs=pl.BlockSpec(memory_space=pltpu.VMEM),
        scratch_shapes=[
            pltpu.VMEM((tokens, cols), BF16),
            pltpu.VMEM((2, 1, cols), F32),
            pltpu.VMEM((2, cols, hidden), F32),
            pltpu.VMEM((cols, hidden), BF16),
            pltpu.VMEM((2, hidden, cols), F32),
            pltpu.VMEM((2, n, block, cols), BF16),
            pltpu.VMEM((2, n, tokens, block), BF16),
            pltpu.VMEM((2, n, tokens, block), BF16),
            pltpu.VMEM((2, ROWS, tokens), F32),
            pltpu.VMEM((2, n, ROWS, tokens), F32),
            pltpu.VMEM((2, n, tokens, block), BF16),
            pltpu.VMEM((2, m, tokens, cols), BF16),
            dma((7,)),
            dma((2, n)), dma((2, n)),
            dma((2, n)), dma((2, n)),
            dma((2, n)), dma((2, n)),
            dma((2, m)), dma((2, m)),
        ],
        compiler_params=pltpu.CompilerParams(
            collective_id=0, has_side_effects=True
        ),
    )(
        stream, gain_first.reshape(1, cols), up_first, down_first,
        gain_second.reshape(1, cols), up_second, down_second,
    )


def solution(mesh):
    return jax.shard_map(
        functools.partial(local, mesh.shape["ra"], mesh.shape["cb"]),
        mesh=mesh,
        in_specs=(
            P(None, "ra"),
            P("ra"),
            P("ra", "cb"),
            P("cb", "ra"),
            P("ra"),
            P("ra", "cb"),
            P("cb", "ra"),
        ),
        out_specs=P(None, "ra"),
        check_vma=False,
    )
```

profile of v0, /device:TPU:1, one launch (start us, length us, event | category | flops | bytes accessed | tf_op | source)
XLA Modules:
  0.0 90.9 jit_solution(2254091927400994428)
XLA Ops:
  0.0 1.4 %copy.8.stream_hbm = bf16[64,32]{1,0:T(8,128)(2,1)} copy(bf16[64,32]{0,1:T(8,128)(2,1)} %param.7) | data formatting | bytes 8192 | tf_op args[0]
  1.4 0.0 copy-start
  1.4 1.7 %copy.9.down1_hbm = f32[512,32]{1,0:T(8,128)} copy(f32[512,32]{0,1:T(8,128)} %param.10) | data formatting | bytes 131072 | tf_op args[3]
  3.1 0.0 copy-done
  3.1 0.8 copy.10.down2_hbm
  3.9 85.6 %shard_map.73 = bf16[64,32]{1,0:T(8,128)(2,1)} custom-call(bf16[64,32]{1,0:T(8,128)(2,1)} %copy.8.stream_hbm, f32[1,32]{1,0:T(1,128)} %bitcast.2, f32[32,512]{1,0:T(8,128)} %up1_hbm.1, f32[512,32]{1,0:T(8,128)} %copy.9.down1_hbm, f32[1,32]{1,0:T(1,128)} %bitcast.3, f32[32,512]{1,0:T(8,128)} %up2_hbm.1, f32[512,32]{1,0:T(8,128)} %copy.10.down2_hbm), custom_call_target="tpu_custom_call" | custom-call | tf_op jit(solution)/shard_map/pallas_call | solution.py:189
  89.5 1.4 %copy.11 = bf16[64,32]{0,1:T(8,128)(2,1)} copy(bf16[64,32]{1,0:T(8,128)(2,1)} %shard_map.73) | data formatting | bytes 8192 | tf_op jit(solution)/shard_map/pallas_call | solution.py:189
Async XLA Ops:
  1.4 1.7 %copy-start = (f32[512,32]{0,1:T(8,128)S(1)}, f32[512,32]{0,1:T(8,128)}, u32[]{:S(2)}) copy-start(f32[512,32]{0,1:T(8,128)} %param.13) | copy-start | bytes 196612
where the time goes:
time: 91.2 us; the launch traced here: 90.9 us
  Pallas kernels  85.6 us (94%)
  local copies, waits for them, and re-layouts  5.3 us (6%)
    pallas_call x1, Pallas kernels, local(): pl.pallas_call(functools.partial(kernel, n, m, cols * n), out_shape=jax.S...  85.6 us
    unnamed x5, local copies, waits for them, and re-layouts  3.91 us

commit v1 on v0

v1 whole, which is shorter than its diff:
```python
import functools

import jax
import jax.numpy as jnp
from jax import lax
from jax.experimental import pallas as pl
from jax.experimental.pallas import tpu as pltpu
from jax.sharding import PartitionSpec as P

NZ, NY, NX = 8, 4, 4
EPS = 1e-06
RESIDUAL = 0.25
LANES = 128
MESH = pl.DeviceIdType.MESH
F32 = jnp.float32
BF16 = jnp.bfloat16
NT = (((1,), (1,)), ((), ()))


def ring(offset, size):
    return min(offset, size - offset)


def farthest_first(offsets):
    return sorted(
        offsets, key=lambda o: (-(ring(o[0], NZ) + ring(o[1], NY) + ring(o[2], NX)), o))


ROW = farthest_first([(0, k, 0) for k in range(1, NY)])
COLUMN = farthest_first([(k, 0, 0) for k in range(1, NZ)])
PLANE = farthest_first([(0, j, k) for j in range(NY) for k in range(NX) if j or k])


def kernel(
    width,
    stream_hbm, gain1_hbm, up1_hbm, down1_hbm, gain2_hbm, up2_hbm, down2_hbm,
    out_ref,
    gain_v, up_v, down_v, stage, wall, ut, pre, sq, branch, fin, fin_in,
    load_sem, w_ss, w_rs, u_ss, u_rs, pre_ss, pre_rs, sq_ss, sq_rs, br_ss, br_rs,
    fin_ss, fin_rs, fin_ss0,
):
    ra = lax.axis_index("ra")
    cb = lax.axis_index("cb")
    z, y = lax.div(ra, NY), lax.rem(ra, NY)
    x, core = lax.div(cb, 2), lax.rem(cb, 2)
    here = y * NX + x
    tokens = ut.shape[-1]
    cols = ut.shape[1]

    def device(offset, at_core):
        dz, dy, dx = offset
        to_z = lax.rem(z + dz, NZ) if dz else z
        to_y = lax.rem(y + dy, NY) if dy else y
        to_x = lax.rem(x + dx, NX) if dx else x
        return {"ra": to_z * NY + to_y, "cb": to_x * 2 + at_core}

    def send(src, dst, ss, rs, offset, at_core):
        pltpu.make_async_remote_copy(
            src_ref=src, dst_ref=dst, send_sem=ss, recv_sem=rs,
            device_id=device(offset, at_core), device_id_type=MESH,
        ).start()

    def arrived(ref, rs):
        pltpu.make_async_copy(ref, ref, rs).wait()

    loads = [
        pltpu.make_async_copy(src, dst, load_sem.at[i])
        for i, (src, dst) in enumerate((
            (gain1_hbm, gain_v.at[0]),
            (up1_hbm, up_v.at[0]),
            (down1_hbm, down_v.at[0]),
            (gain2_hbm, gain_v.at[1]),
            (up2_hbm, up_v.at[1]),
            (down2_hbm, down_v.at[1]),
        ))
    ]
    load_u = pltpu.make_async_copy(stream_hbm, ut.at[y], load_sem.at[6])
    barrier = pltpu.get_barrier_semaphore()

    def hello(offset, at_core):
        pl.semaphore_signal(
            barrier, inc=1, device_id=device(offset, at_core), device_id_type=MESH)

    def place(which, layer):
        if which == 0:
            column = jnp.broadcast_to(gain_v[layer], (LANES, cols)).T[:, :1]
            rows = (up_v[layer] * column).astype(BF16)
        else:
            rows = down_v[layer].astype(BF16)
        for j in range(NY):
            stage[2 * layer + which, j] = rows[:, j * LANES:(j + 1) * LANES]

    def wait_weights(which, layer):
        if which == 0:
            loads[3 * layer].wait()
            loads[3 * layer + 1].wait()
        else:
            loads[3 * layer + 2].wait()

    loads[0].start()
    loads[1].start()

    @pl.when(core == 1)
    def _():
        load_u.start()
        for offset in COLUMN + PLANE:
            hello(offset, 1)
        for offset in [(0, 0, 0)] + PLANE:
            hello(offset, 0)
        for load in loads[2:]:
            load.start()
        wait_weights(0, 0)
        place(0, 0)
        wall[0, NY + y] = stage[0, y]
        load_u.wait()
        pl.semaphore_wait(barrier, len(COLUMN) + len(PLANE) + NX * NY)

        for offset in ROW:
            send(ut.at[y], ut.at[y], u_ss, u_rs, offset, 1)
        for m in range(4):
            which, layer = m % 2, m // 2
            if m:
                wait_weights(which, layer)
                place(which, layer)
                wall[m, NY + y] = stage[m, y]
            for offset in ROW:
                peer = lax.rem(y + offset[1], NY)
                send(stage.at[m, peer], wall.at[m, NY + y], w_ss.at[m], w_rs.at[m], offset, 1)

        arrived(ut.at[pl.ds(0, NY - 1)], u_rs)
        u_t = ut[...].reshape(NY * cols, tokens).astype(F32)
        floated = u_t.T
        scaled = floated
        result_t = None
        for layer in range(2):
            sq[layer, z] = jnp.sum(u_t * u_t, axis=0, keepdims=True)
            arrived(wall.at[2 * layer, pl.ds(0, 2 * NY - 1)], w_rs.at[2 * layer])
            lhs = floated.astype(BF16)
            for c in range(2):
                up = wall[2 * layer, c * NY:(c + 1) * NY].reshape(NY * cols, LANES)
                part = jnp.dot(lhs, up, preferred_element_type=F32)
                pre[layer, z, c] = part.astype(BF16)
            for offset in COLUMN:
                send(pre.at[layer, z], pre.at[layer, z], pre_ss.at[layer], pre_rs.at[layer], offset, 1)
            for offset in COLUMN:
                send(sq.at[layer, z], sq.at[layer, z], sq_ss.at[layer], sq_rs.at[layer], offset, 1)
            arrived(wall.at[2 * layer + 1, pl.ds(0, 2 * NY - 1)], w_rs.at[2 * layer + 1])
            if layer == 1:
                residual = u_t * (RESIDUAL / (NX * NY))

            arrived(pre.at[layer, pl.ds(0, NZ - 1)], pre_rs.at[layer])
            acts = []
            for c in range(2):
                total = pre[layer, 0, c].astype(F32)
                for j in range(1, NZ):
                    total += pre[layer, j, c].astype(F32)
                positive = jnp.maximum(total, 0.0)
                acts.append((positive * positive).astype(BF16))
            downs = [
                wall[2 * layer + 1, c * NY:(c + 1) * NY].reshape(NY * cols, LANES)
                for c in range(2)
            ]
            if layer == 0:
                out = sum(
                    lax.dot_general(a, w, NT, preferred_element_type=F32)
                    for a, w in zip(acts, downs))
                branch[here] = out.astype(BF16)
                for offset in PLANE:
                    send(branch.at[here], branch.at[here], br_ss, br_rs, offset, 1)
            arrived(sq.at[layer, pl.ds(0, NZ - 1)], sq_rs.at[layer])
            squares = sq[layer, 0]
            for j in range(1, NZ):
                squares += sq[layer, j]
            factor = 1.0 / (squares / width + EPS)
            if layer == 0:
                scale = jnp.broadcast_to(factor, (LANES, tokens)).T
                arrived(branch.at[pl.ds(0, NX * NY - 1)], br_rs)
                total = branch[0].astype(F32)
                for j in range(1, NX * NY):
                    total += branch[j].astype(F32)
                floated = (RESIDUAL * floated + total * scale).astype(BF16).astype(F32)
                u_t = floated.T
            else:
                out = sum(
                    lax.dot_general(w, a, NT, preferred_element_type=F32)
                    for a, w in zip(acts, downs))
                out = (out * factor + residual).astype(BF16)
                for j in range(NY):
                    fin[j] = out[j * cols:(j + 1) * cols]
                for offset in PLANE:
                    peer = lax.rem(y + offset[1], NY)
                    send(fin.at[peer], fin_in.at[here], fin_ss0, fin_rs, offset, 0)
                    send(fin.at[peer], fin_in.at[here], fin_ss, fin_rs, offset, 1)
                send(fin.at[y], fin_in.at[here], fin_ss0, fin_rs, (0, 0, 0), 0)
                fin_in[here] = fin[y]
        arrived(fin_in.at[pl.ds(0, NX * NY - 1)], fin_rs)

    @pl.when(core == 0)
    def _():
        for offset in [(0, 0, 0)] + PLANE:
            hello(offset, 1)
        for load in loads[2:]:
            load.start()
        wait_weights(0, 0)
        place(0, 0)
        pl.semaphore_wait(barrier, NX * NY)
        for m in range(4):
            which, layer = m % 2, m // 2
            if m:
                wait_weights(which, layer)
                place(which, layer)
            for offset in ROW + [(0, 0, 0)]:
                peer = lax.rem(y + offset[1], NY)
                send(stage.at[m, peer], wall.at[m, y], w_ss.at[m], w_rs.at[m], offset, 1)
        for m in range(4):
            arrived(stage.at[m], w_ss.at[m])
        arrived(fin_in, fin_rs)

    total = fin_in[0].astype(F32)
    for j in range(1, NX * NY):
        total += fin_in[j].astype(F32)
    out_ref[...] = total.astype(BF16)

    @pl.when(core == 1)
    def _():
        arrived(ut.at[pl.ds(0, NY - 1)], u_ss)
        for m in range(4):
            arrived(stage.at[m, pl.ds(0, NY - 1)], w_ss.at[m])
        for layer in range(2):
            arrived(pre.at[layer, pl.ds(0, NZ - 1)], pre_ss.at[layer])
            arrived(sq.at[layer, pl.ds(0, NZ - 1)], sq_ss.at[layer])
        arrived(branch.at[pl.ds(0, NX * NY - 1)], br_ss)
        arrived(fin_in.at[pl.ds(0, NX * NY - 1)], fin_ss)
        arrived(fin_in, fin_ss0)


def local(stream, gain_first, up_first, down_first, gain_second, up_second, down_second):
    tokens, cols = stream.shape
    hidden = up_first.shape[1]
    dma = pltpu.SemaphoreType.DMA
    out = pl.pallas_call(
        functools.partial(kernel, cols * NZ * NY),
        out_shape=jax.ShapeDtypeStruct((cols, tokens), BF16),
        in_specs=[pl.BlockSpec(memory_space=pl.ANY)] * 7,
        out_specs=pl.BlockSpec(memory_space=pltpu.VMEM),
        scratch_shapes=[
            pltpu.VMEM((2, 1, cols), F32),
            pltpu.VMEM((2, cols, hidden), F32),
            pltpu.VMEM((2, cols, hidden), F32),
            pltpu.VMEM((4, NY, cols, LANES), BF16),
            pltpu.VMEM((4, 2 * NY, cols, LANES), BF16),
            pltpu.VMEM((NY, cols, tokens), BF16),
            pltpu.VMEM((2, NZ, 2, tokens, LANES), BF16),
            pltpu.VMEM((2, NZ, 1, tokens), F32),
            pltpu.VMEM((NX * NY, tokens, LANES), BF16),
            pltpu.VMEM((NY, cols, tokens), BF16),
            pltpu.VMEM((NX * NY, cols, tokens), BF16),
            dma((7,)),
            dma((4,)), dma((4,)),
            dma, dma,
            dma((2,)), dma((2,)),
            dma((2,)), dma((2,)),
            dma, dma,
            dma, dma, dma,
        ],
        compiler_params=pltpu.CompilerParams(
            collective_id=0, has_side_effects=True
        ),
    )(
        stream.T, gain_first.reshape(1, cols), up_first, down_first.T,
        gain_second.reshape(1, cols), up_second, down_second.T,
    )
    return out.T


def solution(mesh):
    return jax.shard_map(
        local,
        mesh=mesh,
        in_specs=(
            P(None, "ra"),
            P("ra"),
            P("ra", "cb"),
            P("cb", "ra"),
            P("ra"),
            P("ra", "cb"),
            P("cb", "ra"),
        ),
        out_specs=P(None, "ra"),
        check_vma=False,
    )
```

time: 91.2 us -> 36.3 us (0.40)
  Pallas kernels: 85.6 us -> 34.8 us
  local copies, waits for them, and re-layouts: 5.3 us -> 1.3 us
    pallas_call x1, Pallas kernels: 85.6 us -> 34.8 us  [local(): pl.pallas_call(functools.partial(kernel, cols * NZ * NY), out_shape=jax.S...]
    unnamed x5 -> x1, local copies, waits for them, and re-layouts: 3.91 us -> 1.3 us
    pallas_call x1 -> x0, local copies, waits for them, and re-layouts: 1.39 us -> none  [local(): pl.pallas_call(functools.partial(kernel, n, m, cols * n), out_shape=jax.S...]
where the time goes in v1:
time: 36.3 us; the launch traced here: 36.1 us
  Pallas kernels  34.8 us (96%)
  local copies, waits for them, and re-layouts  1.3 us (4%)
    pallas_call x1, Pallas kernels, local(): pl.pallas_call(functools.partial(kernel, cols * NZ * NY), out_shape=jax.S...  34.8 us
    unnamed x1, local copies, waits for them, and re-layouts  1.3 us

profile of v1, /device:TPU:1, one launch (start us, length us, event | category | flops | bytes accessed | tf_op | source)
XLA Modules:
  0.0 36.1 jit_solution(11742714040259322131)
XLA Ops:
  0.0 34.8 %shard_map.73 = bf16[32,64]{1,0:T(8,128)(2,1)} custom-call(bf16[32,64]{1,0:T(8,128)(2,1)} %bitcast.9, f32[1,32]{1,0:T(1,128)} %bitcast.10, f32[32,512]{1,0:T(8,128)} %up1_hbm.1, f32[32,512]{1,0:T(8,128)} %bitcast.6, f32[1,32]{1,0:T(1,128)} %bitcast.11, f32[32,512]{1,0:T(8,128)} %up2_hbm.1, f32[32,512]{1,0:T(8,128)} %bitcast.7), custom_call_target="tpu_custom_call" | custom-call | tf_op jit(solution)/shard_map/pallas_call | solution.py:241
  34.8 1.3 %copy.9 = bf16[64,32]{0,1:T(8,128)(2,1)} copy(bf16[64,32]{0,1:T(8,128)(2,1)} %bitcast.8) | data formatting | bytes 8192

commit v2 on v1

v2 whole, which is shorter than its diff:
```python
import functools

import jax
import jax.numpy as jnp
from jax import lax
from jax.experimental import pallas as pl
from jax.experimental.pallas import tpu as pltpu
from jax.sharding import PartitionSpec as P

NZ, NY, NX = 8, 4, 4
EPS = 1e-06
RESIDUAL = 0.25
LANES = 128
MESH = pl.DeviceIdType.MESH
F32 = jnp.float32
BF16 = jnp.bfloat16
NT = (((1,), (1,)), ((), ()))


def ring(offset, size):
    return min(offset, size - offset)


def farthest_first(offsets):
    return sorted(
        offsets, key=lambda o: (-(ring(o[0], NZ) + ring(o[1], NY) + ring(o[2], NX)), o))


ALONG_Y = farthest_first([(0, k, 0) for k in range(1, NY)])
ALONG_X = farthest_first([(0, 0, k) for k in range(1, NX)])
ALONG_Z = farthest_first([(k, 0, 0) for k in range(1, NZ)])
PLANE = farthest_first([(0, j, k) for j in range(NY) for k in range(NX) if j or k])
HERE = (0, 0, 0)


def kernel(
    width,
    stream_hbm, gain1_hbm, up1_hbm, down1_hbm, gain2_hbm, up2_hbm, down2_hbm,
    out_ref,
    gain_v, up_v, down_v, stage, wall, ut, rows_v, pre, sq, branch, fin,
    load_sem, w_ss, w_rs, u_ss, u_rs, pre_ss, pre_rs, sq_ss, sq_rs, br_ss, br_rs,
    fin_ss, fin_rs, fin_ss0, go, all_in,
):
    ra = lax.axis_index("ra")
    cb = lax.axis_index("cb")
    z, y = lax.div(ra, NY), lax.rem(ra, NY)
    x, core = lax.div(cb, 2), lax.rem(cb, 2)
    here = y * NX + x
    cols, tokens = ut.shape[1:]
    mine = tokens // NY
    half = wall.shape[-1]

    def device(offset, at_core):
        dz, dy, dx = offset
        to_z = lax.rem(z + dz, NZ) if dz else z
        to_y = lax.rem(y + dy, NY) if dy else y
        to_x = lax.rem(x + dx, NX) if dx else x
        return {"ra": to_z * NY + to_y, "cb": to_x * 2 + at_core}

    def send(src, dst, ss, rs, offset, at_core):
        pltpu.make_async_remote_copy(
            src_ref=src, dst_ref=dst, send_sem=ss, recv_sem=rs,
            device_id=device(offset, at_core), device_id_type=MESH,
        ).start()

    def arrived(ref, rs):
        pltpu.make_async_copy(ref, ref, rs).wait()

    def signal(sem, offset, at_core):
        pl.semaphore_signal(
            sem, inc=1, device_id=device(offset, at_core), device_id_type=MESH)

    loads = [
        pltpu.make_async_copy(src, dst, load_sem.at[i])
        for i, (src, dst) in enumerate((
            (gain1_hbm, gain_v.at[0]),
            (up1_hbm, up_v.at[0]),
            (down1_hbm, down_v.at[0]),
            (gain2_hbm, gain_v.at[1]),
            (up2_hbm, up_v.at[1]),
            (down2_hbm, down_v.at[1]),
        ))
    ]
    load_u = pltpu.make_async_copy(stream_hbm, ut.at[y], load_sem.at[6])
    barrier = pltpu.get_barrier_semaphore()

    def weight(m):
        layer = m // 2
        if m % 2 == 0:
            loads[3 * layer].wait()
            loads[3 * layer + 1].wait()
            column = jnp.broadcast_to(gain_v[layer], (LANES, cols)).T[:, :1]
            rows = (up_v[layer] * column).astype(BF16)
        else:
            loads[3 * layer + 2].wait()
            rows = down_v[layer].astype(BF16)
        for h in range(2):
            stage[m, h] = rows[:, h * half:(h + 1) * half]

    def share(m, slot, offsets):
        for h in range(2):
            for offset in offsets:
                send(stage.at[m, h], wall.at[m, h, slot], w_ss.at[m], w_rs.at[m, h], offset, 1)

    loads[0].start()
    loads[1].start()

    @pl.when(core == 1)
    def _():
        load_u.start()
        for offset in ALONG_Y:
            signal(barrier, offset, 1)
        for offset in ALONG_Z + ALONG_X:
            signal(barrier, offset, 0)
        for load in loads[2:]:
            load.start()
        weight(0)
        load_u.wait()
        pl.semaphore_wait(barrier, NY)
        signal(go, HERE, 0)

        for offset in ALONG_Y:
            send(ut.at[y], ut.at[y], u_ss, u_rs, offset, 1)
        for m in range(4):
            if m:
                weight(m)
            share(m, NY + y, ALONG_Y)
            for h in range(2):
                wall[m, h, NY + y] = stage[m, h]

        arrived(ut.at[pl.ds(0, NY - 1)], u_rs)
        rows_v[...] = ut[...].reshape(NY * cols, tokens).astype(F32).T
        floated = rows_v[pl.ds(pl.multiple_of(y * mine, mine), mine)]
        for layer in range(2):
            lhs = floated.astype(BF16)
            for h in range(2):
                arrived(wall.at[2 * layer, h, pl.ds(0, 2 * NY - 1)], w_rs.at[2 * layer, h])
                for c in range(2):
                    up = wall[2 * layer, h, c * NY:(c + 1) * NY].reshape(NY * cols, half)
                    part = jnp.dot(lhs, up, preferred_element_type=F32)
                    pre[layer, h, z, :, c * half:(c + 1) * half] = part.astype(BF16)
                if layer == 0 and h == 0:
                    pl.semaphore_wait(all_in, 1)
                for offset in ALONG_Z:
                    send(pre.at[layer, h, z], pre.at[layer, h, z],
                         pre_ss.at[layer], pre_rs.at[layer, h], offset, 1)
            sq[layer, z] = jnp.sum((floated * floated).T, axis=0, keepdims=True)
            for offset in ALONG_Z:
                send(sq.at[layer, z], sq.at[layer, z], sq_ss.at[layer], sq_rs.at[layer], offset, 1)
            for h in range(2):
                arrived(wall.at[2 * layer + 1, h, pl.ds(0, 2 * NY - 1)], w_rs.at[2 * layer + 1, h])

            total = jnp.zeros((mine, LANES), F32)
            for h in range(2):
                arrived(pre.at[layer, h, pl.ds(0, NZ - 1)], pre_rs.at[layer, h])
                if h == 1:
                    arrived(sq.at[layer, pl.ds(0, NZ - 1)], sq_rs.at[layer])
                preact = pre[layer, h, 0].astype(F32)
                for j in range(1, NZ):
                    preact += pre[layer, h, j].astype(F32)
                positive = jnp.maximum(preact, 0.0)
                act = (positive * positive).astype(BF16)
                for c in range(2):
                    down = wall[2 * layer + 1, h, c * NY:(c + 1) * NY].reshape(NY * cols, half)
                    total += lax.dot_general(
                        act[:, c * half:(c + 1) * half], down, NT, preferred_element_type=F32)
            squares = sq[layer, 0]
            for j in range(1, NZ):
                squares += sq[layer, j]
            factor = 1.0 / (squares / width + EPS)
            scale = jnp.broadcast_to(factor, (LANES, mine)).T

            if layer == 0:
                branch[x] = total.astype(BF16)
                for offset in ALONG_X:
                    send(branch.at[x], branch.at[x], br_ss, br_rs, offset, 1)
                arrived(branch.at[pl.ds(0, NX - 1)], br_rs)
                total = branch[0].astype(F32)
                for j in range(1, NX):
                    total += branch[j].astype(F32)
                floated = (RESIDUAL * floated + total * scale).astype(BF16).astype(F32)
            else:
                fin[here] = (total * scale + floated * (RESIDUAL / NX)).astype(BF16)
                for offset in PLANE:
                    send(fin.at[here], fin.at[here], fin_ss0, fin_rs, offset, 0)
                    send(fin.at[here], fin.at[here], fin_ss, fin_rs, offset, 1)
                send(fin.at[here], fin.at[here], fin_ss0, fin_rs, HERE, 0)
        arrived(fin.at[pl.ds(0, NX * NY - 1)], fin_rs)

    @pl.when(core == 0)
    def _():
        signal(barrier, HERE, 1)
        for load in loads[2:]:
            load.start()
        weight(0)
        pl.semaphore_wait(go, 1)
        for m in range(4):
            if m:
                weight(m)
            share(m, y, ALONG_Y + [HERE])
        pl.semaphore_wait(barrier, NZ - 1 + NX - 1)
        signal(all_in, HERE, 1)
        for m in range(4):
            arrived(wall.at[m, :, pl.ds(0, NY)], w_ss.at[m])
        arrived(fin, fin_rs)

    blocks = []
    for j in range(NY):
        total = fin[j * NX].astype(F32)
        for k in range(1, NX):
            total += fin[j * NX + k].astype(F32)
        blocks.append(total.astype(BF16))
    pick = (
        lax.broadcasted_iota(jnp.int32, (cols, LANES), 1)
        == lax.broadcasted_iota(jnp.int32, (cols, LANES), 0) + y * cols
    ).astype(F32).astype(BF16)
    out_ref[...] = lax.dot_general(
        pick, jnp.concatenate(blocks, axis=0), NT, preferred_element_type=F32).astype(BF16)

    @pl.when(core == 1)
    def _():
        arrived(ut.at[pl.ds(0, NY - 1)], u_ss)
        for m in range(4):
            arrived(wall.at[m, :, pl.ds(0, NY - 1)], w_ss.at[m])
        for layer in range(2):
            arrived(pre.at[layer, :, pl.ds(0, NZ - 1)], pre_ss.at[layer])
            arrived(sq.at[layer, pl.ds(0, NZ - 1)], sq_ss.at[layer])
        arrived(branch.at[pl.ds(0, NX - 1)], br_ss)
        arrived(fin.at[pl.ds(0, NX * NY - 1)], fin_ss)
        arrived(fin, fin_ss0)


def local(stream, gain_first, up_first, down_first, gain_second, up_second, down_second):
    tokens, cols = stream.shape
    hidden = up_first.shape[1]
    mine = tokens // NY
    half = hidden // 2
    dma = pltpu.SemaphoreType.DMA
    operands = [
        pltpu.with_memory_space_constraint(a, pltpu.HBM) for a in (
            stream.T, gain_first.reshape(1, cols), up_first, down_first.T,
            gain_second.reshape(1, cols), up_second, down_second.T)
    ]
    out = pl.pallas_call(
        functools.partial(kernel, cols * NZ * NY),
        out_shape=jax.ShapeDtypeStruct((cols, tokens), BF16),
        in_specs=[pl.BlockSpec(memory_space=pl.ANY)] * 7,
        out_specs=pl.BlockSpec(memory_space=pltpu.VMEM),
        scratch_shapes=[
            pltpu.VMEM((2, 1, cols), F32),
            pltpu.VMEM((2, cols, hidden), F32),
            pltpu.VMEM((2, cols, hidden), F32),
            pltpu.VMEM((4, 2, cols, half), BF16),
            pltpu.VMEM((4, 2, 2 * NY, cols, half), BF16),
            pltpu.VMEM((NY, cols, tokens), BF16),
            pltpu.VMEM((tokens, NY * cols), F32),
            pltpu.VMEM((2, 2, NZ, mine, 2 * half), BF16),
            pltpu.VMEM((2, NZ, 1, mine), F32),
            pltpu.VMEM((NX, mine, LANES), BF16),
            pltpu.VMEM((NX * NY, mine, LANES), BF16),
            dma((7,)),
            dma((4,)), dma((4, 2)),
            dma, dma,
            dma((2,)), dma((2, 2)),
            dma((2,)), dma((2,)),
            dma, dma,
            dma, dma, dma,
            pltpu.SemaphoreType.REGULAR, pltpu.SemaphoreType.REGULAR,
        ],
        compiler_params=pltpu.CompilerParams(
            collective_id=0, has_side_effects=True, vmem_limit_bytes=16 * 1024 * 1024,
        ),
    )(*operands)
    return out.T


def solution(mesh):
    return jax.shard_map(
        local,
        mesh=mesh,
        in_specs=(
            P(None, "ra"),
            P("ra"),
            P("ra", "cb"),
            P("cb", "ra"),
            P("ra"),
            P("ra", "cb"),
            P("cb", "ra"),
        ),
        out_specs=P(None, "ra"),
        check_vma=False,
    )
```

time: 36.3 us -> 32.2 us (0.89)
  Pallas kernels: 34.8 us -> 31.4 us
  local copies, waits for them, and re-layouts: 1.3 us -> 0.6 us
    pallas_call x1, Pallas kernels: 34.8 us -> 31.4 us  [local(): pl.pallas_call(functools.partial(kernel, cols * NZ * NY), out_shape=jax.S...]
    unnamed x1, local copies, waits for them, and re-layouts: 1.3 us -> 0.6 us
where the time goes in v2:
time: 32.2 us; the launch traced here: 32 us
  Pallas kernels  31.4 us (98%)
  local copies, waits for them, and re-layouts  0.6 us (2%)
    pallas_call x1, Pallas kernels, local(): pl.pallas_call(functools.partial(kernel, cols * NZ * NY), out_shape=jax.S...  31.4 us

profile of v2, /device:TPU:1, one launch (start us, length us, event | category | flops | bytes accessed | tf_op | source)
XLA Modules:
  0.0 32.0 jit_solution(16493573834970466590)
XLA Ops:
  0.0 31.4 %shard_map.73 = bf16[32,64]{1,0:T(8,128)(2,1)S(1)} custom-call(bf16[32,64]{1,0:T(8,128)(2,1)} %bitcast.9, f32[1,32]{1,0:T(1,128)} %bitcast.10, f32[32,512]{1,0:T(8,128)} %up1_hbm.1, f32[32,512]{1,0:T(8,128)} %bitcast.7, f32[1,32]{1,0:T(1,128)} %bitcast.11, f32[32,512]{1,0:T(8,128)} %up2_hbm.1, f32[32,512]{1,0:T(8,128)} %bitcast.8), custom_call_target="tpu_custom_call" | custom-call | tf_op jit(solution)/shard_map/pallas_call | solution.py:244
  31.4 0.6 %copy.9 = bf16[64,32]{0,1:T(8,128)(2,1)} copy(bf16[64,32]{0,1:T(8,128)(2,1)S(1)} %bitcast.6) | data formatting | bytes 8192

commit v3 on v2

--- a/solution.py
+++ b/solution.py
@@ -37,9 +37,9 @@
     width,
     stream_hbm, gain1_hbm, up1_hbm, down1_hbm, gain2_hbm, up2_hbm, down2_hbm,
     out_ref,
-    gain_v, up_v, down_v, stage, wall, ut, rows_v, pre, sq, branch, fin,
-    load_sem, w_ss, w_rs, u_ss, u_rs, pre_ss, pre_rs, sq_ss, sq_rs, br_ss, br_rs,
-    fin_ss, fin_rs, fin_ss0, go, all_in,
+    gain_v, up_v, down_v, stage, wall, given, got, ut, rows_v, pre, sq, branch, fin,
+    load_sem, w_ss, w_rs, got_ss, got_rs, u_ss, u_rs, pre_ss, pre_rs, sq_ss, sq_rs,
+    br_ss, br_rs, fin_ss, fin_rs, fin_ss0, go, all_in,
 ):
     ra = lax.axis_index("ra")
     cb = lax.axis_index("cb")
@@ -48,7 +48,6 @@
     here = y * NX + x
     cols, tokens = ut.shape[1:]
     mine = tokens // NY
-    half = wall.shape[-1]
 
     def device(offset, at_core):
         dz, dy, dx = offset
@@ -84,86 +83,101 @@
     load_u = pltpu.make_async_copy(stream_hbm, ut.at[y], load_sem.at[6])
     barrier = pltpu.get_barrier_semaphore()
 
+    def first_products():
+        load_u.wait()
+        loads[0].wait()
+        scaled = (ut[y].astype(F32).T * gain_v[0]).astype(BF16)
+        loads[1].wait()
+        part = jnp.dot(scaled, up_v[0].astype(BF16), preferred_element_type=F32).astype(BF16)
+        for j in range(NY):
+            given[j] = part[j * mine:(j + 1) * mine]
+
+    def share_products(c, offsets):
+        for offset in offsets:
+            peer = lax.rem(y + offset[1], NY)
+            send(given.at[peer], got.at[c, y], got_ss, got_rs.at[c], offset, 1)
+
     def weight(m):
-        layer = m // 2
-        if m % 2 == 0:
-            loads[3 * layer].wait()
-            loads[3 * layer + 1].wait()
-            column = jnp.broadcast_to(gain_v[layer], (LANES, cols)).T[:, :1]
-            rows = (up_v[layer] * column).astype(BF16)
+        if m == 1:
+            loads[3].wait()
+            loads[4].wait()
+            column = jnp.broadcast_to(gain_v[1], (LANES, cols)).T[:, :1]
+            stage[m] = (up_v[1] * column).astype(BF16)
         else:
-            loads[3 * layer + 2].wait()
-            rows = down_v[layer].astype(BF16)
-        for h in range(2):
-            stage[m, h] = rows[:, h * half:(h + 1) * half]
+            loads[2 if m == 0 else 5].wait()
+            stage[m] = down_v[m // 2].astype(BF16)
 
     def share(m, slot, offsets):
-        for h in range(2):
-            for offset in offsets:
-                send(stage.at[m, h], wall.at[m, h, slot], w_ss.at[m], w_rs.at[m, h], offset, 1)
+        for offset in offsets:
+            send(stage.at[m], wall.at[m, slot], w_ss.at[m], w_rs.at[m], offset, 1)
+
+    def whole(m, c):
+        return wall[m, c * NY:(c + 1) * NY].reshape(NY * cols, wall.shape[-1])
 
     loads[0].start()
     loads[1].start()
+    load_u.start()
 
     @pl.when(core == 1)
     def _():
-        load_u.start()
         for offset in ALONG_Y:
             signal(barrier, offset, 1)
         for offset in ALONG_Z + ALONG_X:
             signal(barrier, offset, 0)
         for load in loads[2:]:
             load.start()
-        weight(0)
-        load_u.wait()
+        first_products()
+        got[1, y] = given[y]
         pl.semaphore_wait(barrier, NY)
         signal(go, HERE, 0)
 
+        share_products(1, ALONG_Y)
         for offset in ALONG_Y:
             send(ut.at[y], ut.at[y], u_ss, u_rs, offset, 1)
-        for m in range(4):
-            if m:
-                weight(m)
+        for m in range(3):
+            weight(m)
             share(m, NY + y, ALONG_Y)
-            for h in range(2):
-                wall[m, h, NY + y] = stage[m, h]
-
-        arrived(ut.at[pl.ds(0, NY - 1)], u_rs)
-        rows_v[...] = ut[...].reshape(NY * cols, tokens).astype(F32).T
-        floated = rows_v[pl.ds(pl.multiple_of(y * mine, mine), mine)]
+            wall[m, NY + y] = stage[m]
+
+        floated = None
         for layer in range(2):
-            lhs = floated.astype(BF16)
-            for h in range(2):
-                arrived(wall.at[2 * layer, h, pl.ds(0, 2 * NY - 1)], w_rs.at[2 * layer, h])
-                for c in range(2):
-                    up = wall[2 * layer, h, c * NY:(c + 1) * NY].reshape(NY * cols, half)
-                    part = jnp.dot(lhs, up, preferred_element_type=F32)
-                    pre[layer, h, z, :, c * half:(c + 1) * half] = part.astype(BF16)
-                if layer == 0 and h == 0:
+            for c in (1, 0):
+                if layer == 0:
+                    arrived(got.at[c, pl.ds(0, NY - c)], got_rs.at[c])
+                    part = got[c, 0].astype(F32)
+                    for j in range(1, NY):
+                        part += got[c, j].astype(F32)
+                else:
+                    if c:
+                        arrived(wall.at[1, pl.ds(0, 2 * NY - 1)], w_rs.at[1])
+                    part = jnp.dot(floated.astype(BF16), whole(1, c), preferred_element_type=F32)
+                pre[layer, c, z] = part.astype(BF16)
+                if layer == 0 and c:
                     pl.semaphore_wait(all_in, 1)
                 for offset in ALONG_Z:
-                    send(pre.at[layer, h, z], pre.at[layer, h, z],
-                         pre_ss.at[layer], pre_rs.at[layer, h], offset, 1)
+                    send(pre.at[layer, c, z], pre.at[layer, c, z],
+                         pre_ss.at[layer], pre_rs.at[layer, c], offset, 1)
+            if layer == 0:
+                arrived(ut.at[pl.ds(0, NY - 1)], u_rs)
+                rows_v[...] = ut[...].reshape(NY * cols, tokens).astype(F32).T
+                floated = rows_v[pl.ds(pl.multiple_of(y * mine, mine), mine)]
             sq[layer, z] = jnp.sum((floated * floated).T, axis=0, keepdims=True)
             for offset in ALONG_Z:
                 send(sq.at[layer, z], sq.at[layer, z], sq_ss.at[layer], sq_rs.at[layer], offset, 1)
-            for h in range(2):
-                arrived(wall.at[2 * layer + 1, h, pl.ds(0, 2 * NY - 1)], w_rs.at[2 * layer + 1, h])
+            arrived(wall.at[2 * layer, pl.ds(0, 2 * NY - 1)], w_rs.at[2 * layer])
 
             total = jnp.zeros((mine, LANES), F32)
-            for h in range(2):
-                arrived(pre.at[layer, h, pl.ds(0, NZ - 1)], pre_rs.at[layer, h])
-                if h == 1:
+            for c in (1, 0):
+                arrived(pre.at[layer, c, pl.ds(0, NZ - 1)], pre_rs.at[layer, c])
+                if c == 0:
                     arrived(sq.at[layer, pl.ds(0, NZ - 1)], sq_rs.at[layer])
-                preact = pre[layer, h, 0].astype(F32)
+                preact = pre[layer, c, 0].astype(F32)
                 for j in range(1, NZ):
-                    preact += pre[layer, h, j].astype(F32)
+                    preact += pre[layer, c, j].astype(F32)
                 positive = jnp.maximum(preact, 0.0)
                 act = (positive * positive).astype(BF16)
-                for c in range(2):
-                    down = wall[2 * layer + 1, h, c * NY:(c + 1) * NY].reshape(NY * cols, half)
-                    total += lax.dot_general(
-                        act[:, c * half:(c + 1) * half], down, NT, preferred_element_type=F32)
+                total += lax.dot_general(
+                    act, whole(2 * layer, c), NT, preferred_element_type=F32)
             squares = sq[layer, 0]
             for j in range(1, NZ):
                 squares += sq[layer, j]
@@ -182,9 +196,9 @@
             else:
                 fin[here] = (total * scale + floated * (RESIDUAL / NX)).astype(BF16)
                 for offset in PLANE:
+                    send(fin.at[here], fin.at[here], fin_ss, fin_rs, offset, 1)
+                for offset in PLANE + [HERE]:
                     send(fin.at[here], fin.at[here], fin_ss0, fin_rs, offset, 0)
-                    send(fin.at[here], fin.at[here], fin_ss, fin_rs, offset, 1)
-                send(fin.at[here], fin.at[here], fin_ss0, fin_rs, HERE, 0)
         arrived(fin.at[pl.ds(0, NX * NY - 1)], fin_rs)
 
     @pl.when(core == 0)
@@ -192,16 +206,17 @@
         signal(barrier, HERE, 1)
         for load in loads[2:]:
             load.start()
-        weight(0)
+        first_products()
         pl.semaphore_wait(go, 1)
-        for m in range(4):
-            if m:
-                weight(m)
+        share_products(0, ALONG_Y + [HERE])
+        for m in range(3):
+            weight(m)
             share(m, y, ALONG_Y + [HERE])
         pl.semaphore_wait(barrier, NZ - 1 + NX - 1)
         signal(all_in, HERE, 1)
-        for m in range(4):
-            arrived(wall.at[m, :, pl.ds(0, NY)], w_ss.at[m])
+        arrived(given, got_ss)
+        for m in range(3):
+            arrived(wall.at[m, pl.ds(0, NY)], w_ss.at[m])
         arrived(fin, fin_rs)
 
     blocks = []
@@ -220,8 +235,9 @@
     @pl.when(core == 1)
     def _():
         arrived(ut.at[pl.ds(0, NY - 1)], u_ss)
-        for m in range(4):
-            arrived(wall.at[m, :, pl.ds(0, NY - 1)], w_ss.at[m])
+        arrived(given.at[pl.ds(0, NY - 1)], got_ss)
+        for m in range(3):
+            arrived(wall.at[m, pl.ds(0, NY - 1)], w_ss.at[m])
         for layer in range(2):
             arrived(pre.at[layer, :, pl.ds(0, NZ - 1)], pre_ss.at[layer])
             arrived(sq.at[layer, pl.ds(0, NZ - 1)], sq_ss.at[layer])
@@ -234,7 +250,6 @@
     tokens, cols = stream.shape
     hidden = up_first.shape[1]
     mine = tokens // NY
-    half = hidden // 2
     dma = pltpu.SemaphoreType.DMA
     operands = [
         pltpu.with_memory_space_constraint(a, pltpu.HBM) for a in (
@@ -250,16 +265,19 @@
             pltpu.VMEM((2, 1, cols), F32),
             pltpu.VMEM((2, cols, hidden), F32),
             pltpu.VMEM((2, cols, hidden), F32),
-            pltpu.VMEM((4, 2, cols, half), BF16),
-            pltpu.VMEM((4, 2, 2 * NY, cols, half), BF16),
+            pltpu.VMEM((3, cols, hidden), BF16),
+            pltpu.VMEM((3, 2 * NY, cols, hidden), BF16),
+            pltpu.VMEM((NY, mine, hidden), BF16),
+            pltpu.VMEM((2, NY, mine, hidden), BF16),
             pltpu.VMEM((NY, cols, tokens), BF16),
             pltpu.VMEM((tokens, NY * cols), F32),
-            pltpu.VMEM((2, 2, NZ, mine, 2 * half), BF16),
+            pltpu.VMEM((2, 2, NZ, mine, hidden), BF16),
             pltpu.VMEM((2, NZ, 1, mine), F32),
             pltpu.VMEM((NX, mine, LANES), BF16),
             pltpu.VMEM((NX * NY, mine, LANES), BF16),
             dma((7,)),
-            dma((4,)), dma((4, 2)),
+            dma((3,)), dma((3,)),
+            dma, dma((2,)),
             dma, dma,
             dma((2,)), dma((2, 2)),
             dma((2,)), dma((2,)),

time: 32.2 us -> 31.5 us (0.978)
  Pallas kernels: 31.4 us -> 30.8 us
    pallas_call x1, Pallas kernels: 31.4 us -> 30.8 us  [local(): pl.pallas_call(functools.partial(kernel, cols * NZ * NY), out_shape=jax.S...]
where the time goes in v3:
time: 31.5 us; the launch traced here: 31.4 us
  Pallas kernels  30.8 us (98%)
  local copies, waits for them, and re-layouts  0.6 us (2%)
    pallas_call x1, Pallas kernels, local(): pl.pallas_call(functools.partial(kernel, cols * NZ * NY), out_shape=jax.S...  30.8 us

profile of v3, /device:TPU:1, one launch (start us, length us, event | category | flops | bytes accessed | tf_op | source)
XLA Modules:
  0.0 31.4 jit_solution(4768153629349617610)
XLA Ops:
  0.0 30.8 %shard_map.73 = bf16[32,64]{1,0:T(8,128)(2,1)S(1)} custom-call(bf16[32,64]{1,0:T(8,128)(2,1)} %bitcast.9, f32[1,32]{1,0:T(1,128)} %bitcast.10, f32[32,512]{1,0:T(8,128)} %up1_hbm.1, f32[32,512]{1,0:T(8,128)} %bitcast.7, f32[1,32]{1,0:T(1,128)} %bitcast.11, f32[32,512]{1,0:T(8,128)} %up2_hbm.1, f32[32,512]{1,0:T(8,128)} %bitcast.8), custom_call_target="tpu_custom_call" | custom-call | tf_op jit(solution)/shard_map/pallas_call | solution.py:259
  30.8 0.6 %copy.9 = bf16[64,32]{0,1:T(8,128)(2,1)} copy(bf16[64,32]{0,1:T(8,128)(2,1)S(1)} %bitcast.6) | data formatting | bytes 8192

commit v4 on v3

--- a/solution.py
+++ b/solution.py
@@ -8,6 +8,7 @@
 from jax.sharding import PartitionSpec as P
 
 NZ, NY, NX = 8, 4, 4
+CHUNKS = 4
 EPS = 1e-06
 RESIDUAL = 0.25
 LANES = 128
@@ -29,6 +30,8 @@
 ALONG_Y = farthest_first([(0, k, 0) for k in range(1, NY)])
 ALONG_X = farthest_first([(0, 0, k) for k in range(1, NX)])
 ALONG_Z = farthest_first([(k, 0, 0) for k in range(1, NZ)])
+FAR, NEAR, MIXED = [4, 3, 5, 2, 6, 1, 7], [7, 1, 6, 2, 5, 3, 4], [1, 7, 4, 2, 6, 3, 5]
+Z_ORDERS = [[FAR, FAR, FAR, FAR], [NEAR, NEAR, MIXED, MIXED]]
 PLANE = farthest_first([(0, j, k) for j in range(NY) for k in range(NX) if j or k])
 HERE = (0, 0, 0)
 
@@ -139,45 +142,56 @@
             share(m, NY + y, ALONG_Y)
             wall[m, NY + y] = stage[m]
 
+        def share_squares(layer, u):
+            sq[layer, z] = jnp.sum((u * u).T, axis=0, keepdims=True)
+            for offset in ALONG_Z:
+                send(sq.at[layer, z], sq.at[layer, z], sq_ss.at[layer], sq_rs.at[layer], offset, 1)
+
         floated = None
+        wide = pre.shape[-1]
         for layer in range(2):
-            for c in (1, 0):
-                if layer == 0:
+            for q in range(CHUNKS):
+                c, lane = 1 - q // (CHUNKS // 2), q % (CHUNKS // 2) * wide
+                if layer == 0 and not lane:
                     arrived(got.at[c, pl.ds(0, NY - c)], got_rs.at[c])
                     part = got[c, 0].astype(F32)
                     for j in range(1, NY):
                         part += got[c, j].astype(F32)
-                else:
+                elif not lane:
                     if c:
                         arrived(wall.at[1, pl.ds(0, 2 * NY - 1)], w_rs.at[1])
                     part = jnp.dot(floated.astype(BF16), whole(1, c), preferred_element_type=F32)
-                pre[layer, c, z] = part.astype(BF16)
-                if layer == 0 and c:
+                pre[layer, q, z] = part[:, lane:lane + wide].astype(BF16)
+                if layer == 0 and q == 0:
                     pl.semaphore_wait(all_in, 1)
-                for offset in ALONG_Z:
-                    send(pre.at[layer, c, z], pre.at[layer, c, z],
-                         pre_ss.at[layer], pre_rs.at[layer, c], offset, 1)
+                for k in Z_ORDERS[layer][q]:
+                    send(pre.at[layer, q, z], pre.at[layer, q, z],
+                         pre_ss.at[layer], pre_rs.at[layer, q], (k, 0, 0), 1)
+                if layer == 1 and q == 0:
+                    share_squares(1, floated)
             if layer == 0:
                 arrived(ut.at[pl.ds(0, NY - 1)], u_rs)
                 rows_v[...] = ut[...].reshape(NY * cols, tokens).astype(F32).T
                 floated = rows_v[pl.ds(pl.multiple_of(y * mine, mine), mine)]
-            sq[layer, z] = jnp.sum((floated * floated).T, axis=0, keepdims=True)
-            for offset in ALONG_Z:
-                send(sq.at[layer, z], sq.at[layer, z], sq_ss.at[layer], sq_rs.at[layer], offset, 1)
+                share_squares(0, floated)
             arrived(wall.at[2 * layer, pl.ds(0, 2 * NY - 1)], w_rs.at[2 * layer])
 
             total = jnp.zeros((mine, LANES), F32)
-            for c in (1, 0):
-                arrived(pre.at[layer, c, pl.ds(0, NZ - 1)], pre_rs.at[layer, c])
-                if c == 0:
-                    arrived(sq.at[layer, pl.ds(0, NZ - 1)], sq_rs.at[layer])
-                preact = pre[layer, c, 0].astype(F32)
+            for q in range(CHUNKS):
+                c, lane = 1 - q // (CHUNKS // 2), q % (CHUNKS // 2) * wide
+                arrived(pre.at[layer, q, pl.ds(0, NZ - 1)], pre_rs.at[layer, q])
+                preact = pre[layer, q, 0].astype(F32)
                 for j in range(1, NZ):
-                    preact += pre[layer, c, j].astype(F32)
+                    preact += pre[layer, q, j].astype(F32)
                 positive = jnp.maximum(preact, 0.0)
                 act = (positive * positive).astype(BF16)
                 total += lax.dot_general(
-                    act, whole(2 * layer, c), NT, preferred_element_type=F32)
+                    act, whole(2 * layer, c)[:, lane:lane + wide], NT, preferred_element_type=F32)
+            if layer == 0:
+                branch[x] = total.astype(BF16)
+                for offset in ALONG_X:
+                    send(branch.at[x], branch.at[x], br_ss, br_rs, offset, 1)
+            arrived(sq.at[layer, pl.ds(0, NZ - 1)], sq_rs.at[layer])
             squares = sq[layer, 0]
             for j in range(1, NZ):
                 squares += sq[layer, j]
@@ -185,9 +199,6 @@
             scale = jnp.broadcast_to(factor, (LANES, mine)).T
 
             if layer == 0:
-                branch[x] = total.astype(BF16)
-                for offset in ALONG_X:
-                    send(branch.at[x], branch.at[x], br_ss, br_rs, offset, 1)
                 arrived(branch.at[pl.ds(0, NX - 1)], br_rs)
                 total = branch[0].astype(F32)
                 for j in range(1, NX):
@@ -271,7 +282,7 @@
             pltpu.VMEM((2, NY, mine, hidden), BF16),
             pltpu.VMEM((NY, cols, tokens), BF16),
             pltpu.VMEM((tokens, NY * cols), F32),
-            pltpu.VMEM((2, 2, NZ, mine, hidden), BF16),
+            pltpu.VMEM((2, CHUNKS, NZ, mine, 2 * hidden // CHUNKS), BF16),
             pltpu.VMEM((2, NZ, 1, mine), F32),
             pltpu.VMEM((NX, mine, LANES), BF16),
             pltpu.VMEM((NX * NY, mine, LANES), BF16),
@@ -279,7 +290,7 @@
             dma((3,)), dma((3,)),
             dma, dma((2,)),
             dma, dma,
-            dma((2,)), dma((2, 2)),
+            dma((2,)), dma((2, CHUNKS)),
             dma((2,)), dma((2,)),
             dma, dma,
             dma, dma, dma,

time: 31.5 us -> 29.9 us (0.949)
  Pallas kernels: 30.8 us -> 29.2 us
    pallas_call x1, Pallas kernels: 30.8 us -> 29.2 us  [local(): pl.pallas_call(functools.partial(kernel, cols * NZ * NY), out_shape=jax.S...]
where the time goes in v4:
time: 29.9 us; the launch traced here: 29.8 us
  Pallas kernels  29.2 us (98%)
  local copies, waits for them, and re-layouts  0.6 us (2%)
    pallas_call x1, Pallas kernels, local(): pl.pallas_call(functools.partial(kernel, cols * NZ * NY), out_shape=jax.S...  29.2 us
    unnamed x1, local copies, waits for them, and re-layouts  0.6 us

profile of v4, /device:TPU:1, one launch (start us, length us, event | category | flops | bytes accessed | tf_op | source)
XLA Modules:
  0.0 29.8 jit_solution(4973160583656039416)
XLA Ops:
  0.0 29.2 %shard_map.73 = bf16[32,64]{1,0:T(8,128)(2,1)S(1)} custom-call(bf16[32,64]{1,0:T(8,128)(2,1)} %bitcast.9, f32[1,32]{1,0:T(1,128)} %bitcast.10, f32[32,512]{1,0:T(8,128)} %up1_hbm.1, f32[32,512]{1,0:T(8,128)} %bitcast.7, f32[1,32]{1,0:T(1,128)} %bitcast.11, f32[32,512]{1,0:T(8,128)} %up2_hbm.1, f32[32,512]{1,0:T(8,128)} %bitcast.8), custom_call_target="tpu_custom_call" | custom-call | tf_op jit(solution)/shard_map/pallas_call | solution.py:270
  29.2 0.6 %copy.9 = bf16[64,32]{0,1:T(8,128)(2,1)} copy(bf16[64,32]{0,1:T(8,128)(2,1)S(1)} %bitcast.6) | data formatting | bytes 8192

commit v5 on v4

--- a/solution.py
+++ b/solution.py
@@ -30,8 +30,7 @@
 ALONG_Y = farthest_first([(0, k, 0) for k in range(1, NY)])
 ALONG_X = farthest_first([(0, 0, k) for k in range(1, NX)])
 ALONG_Z = farthest_first([(k, 0, 0) for k in range(1, NZ)])
-FAR, NEAR, MIXED = [4, 3, 5, 2, 6, 1, 7], [7, 1, 6, 2, 5, 3, 4], [1, 7, 4, 2, 6, 3, 5]
-Z_ORDERS = [[FAR, FAR, FAR, FAR], [NEAR, NEAR, MIXED, MIXED]]
+LATER_Z = [1, 7, 2, 6, 3, 5, 4]
 PLANE = farthest_first([(0, j, k) for j in range(NY) for k in range(NX) if j or k])
 HERE = (0, 0, 0)
 
@@ -42,7 +41,7 @@
     out_ref,
     gain_v, up_v, down_v, stage, wall, given, got, ut, rows_v, pre, sq, branch, fin,
     load_sem, w_ss, w_rs, got_ss, got_rs, u_ss, u_rs, pre_ss, pre_rs, sq_ss, sq_rs,
-    br_ss, br_rs, fin_ss, fin_rs, fin_ss0, go, all_in,
+    br_ss, br_rs, fin_ss, fin_rs, fin_ss0, go, all_in, first_ss,
 ):
     ra = lax.axis_index("ra")
     cb = lax.axis_index("cb")
@@ -141,6 +140,20 @@
             weight(m)
             share(m, NY + y, ALONG_Y)
             wall[m, NY + y] = stage[m]
+
+        def send_second(to_z, q, ss):
+            @pl.when(z != to_z)
+            def _():
+                pltpu.make_async_remote_copy(
+                    src_ref=pre.at[1, q, z], dst_ref=pre.at[1, q, z],
+                    send_sem=ss, recv_sem=pre_rs.at[1, q],
+                    device_id={"ra": to_z * NY + y, "cb": x * 2 + 1}, device_id_type=MESH,
+                ).start()
+
+        def sent_second(to_z, ss):
+            @pl.when(z != to_z)
+            def _():
+                arrived(pre.at[1, :, 0], ss)
 
         def share_squares(layer, u):
             sq[layer, z] = jnp.sum((u * u).T, axis=0, keepdims=True)
@@ -164,21 +177,39 @@
                 pre[layer, q, z] = part[:, lane:lane + wide].astype(BF16)
                 if layer == 0 and q == 0:
                     pl.semaphore_wait(all_in, 1)
-                for k in Z_ORDERS[layer][q]:
-                    send(pre.at[layer, q, z], pre.at[layer, q, z],
-                         pre_ss.at[layer], pre_rs.at[layer, q], (k, 0, 0), 1)
+                if layer == 0:
+                    for offset in ALONG_Z:
+                        send(pre.at[0, q, z], pre.at[0, q, z],
+                             pre_ss.at[0], pre_rs.at[0, q], offset, 1)
+                else:
+                    send_second(0, q, first_ss)
                 if layer == 1 and q == 0:
                     share_squares(1, floated)
-            if layer == 0:
+            if layer == 1:
+                sent_second(0, first_ss)
+                for to_z in LATER_Z:
+                    for q in range(CHUNKS):
+                        send_second(to_z, q, pre_ss.at[1])
+            else:
                 arrived(ut.at[pl.ds(0, NY - 1)], u_rs)
                 rows_v[...] = ut[...].reshape(NY * cols, tokens).astype(F32).T
                 floated = rows_v[pl.ds(pl.multiple_of(y * mine, mine), mine)]
                 share_squares(0, floated)
             arrived(wall.at[2 * layer, pl.ds(0, 2 * NY - 1)], w_rs.at[2 * layer])
 
+            def scale_of(layer):
+                arrived(sq.at[layer, pl.ds(0, NZ - 1)], sq_rs.at[layer])
+                squares = sq[layer, 0]
+                for j in range(1, NZ):
+                    squares += sq[layer, j]
+                factor = 1.0 / (squares / width + EPS)
+                return jnp.broadcast_to(factor, (LANES, mine)).T
+
             total = jnp.zeros((mine, LANES), F32)
             for q in range(CHUNKS):
                 c, lane = 1 - q // (CHUNKS // 2), q % (CHUNKS // 2) * wide
+                if layer == 1 and q == CHUNKS - 1:
+                    scale = scale_of(1)
                 arrived(pre.at[layer, q, pl.ds(0, NZ - 1)], pre_rs.at[layer, q])
                 preact = pre[layer, q, 0].astype(F32)
                 for j in range(1, NZ):
@@ -191,12 +222,7 @@
                 branch[x] = total.astype(BF16)
                 for offset in ALONG_X:
                     send(branch.at[x], branch.at[x], br_ss, br_rs, offset, 1)
-            arrived(sq.at[layer, pl.ds(0, NZ - 1)], sq_rs.at[layer])
-            squares = sq[layer, 0]
-            for j in range(1, NZ):
-                squares += sq[layer, j]
-            factor = 1.0 / (squares / width + EPS)
-            scale = jnp.broadcast_to(factor, (LANES, mine)).T
+                scale = scale_of(0)
 
             if layer == 0:
                 arrived(branch.at[pl.ds(0, NX - 1)], br_rs)
@@ -249,8 +275,12 @@
         arrived(given.at[pl.ds(0, NY - 1)], got_ss)
         for m in range(3):
             arrived(wall.at[m, pl.ds(0, NY - 1)], w_ss.at[m])
+        arrived(pre.at[0, :, pl.ds(0, NZ - 1)], pre_ss.at[0])
+        for to_z in LATER_Z:
+            @pl.when(z != to_z)
+            def _():
+                arrived(pre.at[1, :, 0], pre_ss.at[1])
         for layer in range(2):
-            arrived(pre.at[layer, :, pl.ds(0, NZ - 1)], pre_ss.at[layer])
             arrived(sq.at[layer, pl.ds(0, NZ - 1)], sq_ss.at[layer])
         arrived(branch.at[pl.ds(0, NX - 1)], br_ss)
         arrived(fin.at[pl.ds(0, NX * NY - 1)], fin_ss)
@@ -294,7 +324,7 @@
             dma((2,)), dma((2,)),
             dma, dma,
             dma, dma, dma,
-            pltpu.SemaphoreType.REGULAR, pltpu.SemaphoreType.REGULAR,
+            pltpu.SemaphoreType.REGULAR, pltpu.SemaphoreType.REGULAR, dma,
         ],
         compiler_params=pltpu.CompilerParams(
             collective_id=0, has_side_effects=True, vmem_limit_bytes=16 * 1024 * 1024,

time: 29.9 us -> 29.2 us (0.977)
  Pallas kernels: 29.2 us -> 28.5 us
    pallas_call x1, Pallas kernels: 29.2 us -> 28.5 us  [local(): pl.pallas_call(functools.partial(kernel, cols * NZ * NY), out_shape=jax.S...]
where the time goes in v5:
time: 29.2 us; the launch traced here: 29.1 us
  Pallas kernels  28.5 us (98%)
  local copies, waits for them, and re-layouts  0.6 us (2%)
    pallas_call x1, Pallas kernels, local(): pl.pallas_call(functools.partial(kernel, cols * NZ * NY), out_shape=jax.S...  28.5 us
    unnamed x1, local copies, waits for them, and re-layouts  0.6 us

profile of v5, /device:TPU:1, one launch (start us, length us, event | category | flops | bytes accessed | tf_op | source)
XLA Modules:
  0.0 29.1 jit_solution(296621435784534828)
XLA Ops:
  0.0 28.5 %shard_map.73 = bf16[32,64]{1,0:T(8,128)(2,1)S(1)} custom-call(bf16[32,64]{1,0:T(8,128)(2,1)} %bitcast.9, f32[1,32]{1,0:T(1,128)} %bitcast.10, f32[32,512]{1,0:T(8,128)} %up1_hbm.1, f32[32,512]{1,0:T(8,128)} %bitcast.7, f32[1,32]{1,0:T(1,128)} %bitcast.11, f32[32,512]{1,0:T(8,128)} %up2_hbm.1, f32[32,512]{1,0:T(8,128)} %bitcast.8), custom_call_target="tpu_custom_call" | custom-call | tf_op jit(solution)/shard_map/pallas_call | solution.py:300
  28.5 0.6 %copy.9 = bf16[64,32]{0,1:T(8,128)(2,1)} copy(bf16[64,32]{0,1:T(8,128)(2,1)S(1)} %bitcast.6) | data formatting | bytes 8192

commit v6 on v5

--- a/solution.py
+++ b/solution.py
@@ -30,7 +30,8 @@
 ALONG_Y = farthest_first([(0, k, 0) for k in range(1, NY)])
 ALONG_X = farthest_first([(0, 0, k) for k in range(1, NX)])
 ALONG_Z = farthest_first([(k, 0, 0) for k in range(1, NZ)])
-LATER_Z = [1, 7, 2, 6, 3, 5, 4]
+FIRST_Z = [[4, 3, 5, 2, 6, 1, 7], [3, 5, 2, 4, 6, 1, 7], [4, 5, 3, 2, 6, 1, 7], [4, 3, 5, 2, 6, 1, 7]]
+LATER_Z = [1, 2, 7, 6, 3, 4, 5]
 PLANE = farthest_first([(0, j, k) for j in range(NY) for k in range(NX) if j or k])
 HERE = (0, 0, 0)
 
@@ -178,9 +179,9 @@
                 if layer == 0 and q == 0:
                     pl.semaphore_wait(all_in, 1)
                 if layer == 0:
-                    for offset in ALONG_Z:
+                    for k in FIRST_Z[q]:
                         send(pre.at[0, q, z], pre.at[0, q, z],
-                             pre_ss.at[0], pre_rs.at[0, q], offset, 1)
+                             pre_ss.at[0], pre_rs.at[0, q], (k, 0, 0), 1)
                 else:
                     send_second(0, q, first_ss)
                 if layer == 1 and q == 0:

time: 29.2 us -> 28.8 us (0.986)
  the two profiles are of different devices: /device:TPU:1 before, /device:TPU:32 now
where the time goes in v6:
time: 28.8 us; the launch traced here: 28.7 us
  Pallas kernels  28.1 us (98%)
  local copies, waits for them, and re-layouts  0.6 us (2%)
    pallas_call x1, Pallas kernels, local(): pl.pallas_call(functools.partial(kernel, cols * NZ * NY), out_shape=jax.S...  28.1 us
    unnamed x1, local copies, waits for them, and re-layouts  0.6 us

profile of v6, /device:TPU:32, one launch (start us, length us, event | category | flops | bytes accessed | tf_op | source)
XLA Modules:
  0.0 28.7 jit_solution(9100653446203675117)
XLA Ops:
  0.0 28.1 %shard_map.73 = bf16[32,64]{1,0:T(8,128)(2,1)S(1)} custom-call(bf16[32,64]{1,0:T(8,128)(2,1)} %bitcast.9, f32[1,32]{1,0:T(1,128)} %bitcast.10, f32[32,512]{1,0:T(8,128)} %up1_hbm.1, f32[32,512]{1,0:T(8,128)} %bitcast.7, f32[1,32]{1,0:T(1,128)} %bitcast.11, f32[32,512]{1,0:T(8,128)} %up2_hbm.1, f32[32,512]{1,0:T(8,128)} %bitcast.8), custom_call_target="tpu_custom_call" | custom-call | tf_op jit(solution)/shard_map/pallas_call | solution.py:301
  28.1 0.6 %copy.9 = bf16[64,32]{0,1:T(8,128)(2,1)} copy(bf16[64,32]{0,1:T(8,128)(2,1)S(1)} %bitcast.6) | data formatting | bytes 8192

commit v7 on v6

--- a/solution.py
+++ b/solution.py
@@ -123,9 +123,11 @@
 
     @pl.when(core == 1)
     def _():
+        for offset in ALONG_Z[:3]:
+            signal(barrier, offset, 0)
         for offset in ALONG_Y:
             signal(barrier, offset, 1)
-        for offset in ALONG_Z + ALONG_X:
+        for offset in ALONG_Z[3:] + ALONG_X:
             signal(barrier, offset, 0)
         for load in loads[2:]:
             load.start()
@@ -247,11 +249,13 @@
         first_products()
         pl.semaphore_wait(go, 1)
         share_products(0, ALONG_Y + [HERE])
-        for m in range(3):
+        weight(0)
+        share(0, y, ALONG_Y + [HERE])
+        pl.semaphore_wait(barrier, NZ - 1 + NX - 1)
+        signal(all_in, HERE, 1)
+        for m in (1, 2):
             weight(m)
             share(m, y, ALONG_Y + [HERE])
-        pl.semaphore_wait(barrier, NZ - 1 + NX - 1)
-        signal(all_in, HERE, 1)
         arrived(given, got_ss)
         for m in range(3):
             arrived(wall.at[m, pl.ds(0, NY)], w_ss.at[m])

time: 28.8 us -> 28.6 us (level)
  the two profiles are of different devices: /device:TPU:32 before, /device:TPU:1 now
where the time goes in v7:
time: 28.6 us; the launch traced here: 28.1 us
  Pallas kernels  27.5 us (96%)
  local copies, waits for them, and re-layouts  0.6 us (2%)
    pallas_call x1, Pallas kernels, local(): pl.pallas_call(functools.partial(kernel, cols * NZ * NY), out_shape=jax.S...  27.5 us
    unnamed x1, local copies, waits for them, and re-layouts  0.6 us

profile of v7, /device:TPU:1, one launch (start us, length us, event | category | flops | bytes accessed | tf_op | source)
XLA Modules:
  0.0 28.1 jit_solution(2654725718873576434)
XLA Ops:
  0.0 27.5 %shard_map.73 = bf16[32,64]{1,0:T(8,128)(2,1)S(1)} custom-call(bf16[32,64]{1,0:T(8,128)(2,1)} %bitcast.9, f32[1,32]{1,0:T(1,128)} %bitcast.10, f32[32,512]{1,0:T(8,128)} %up1_hbm.1, f32[32,512]{1,0:T(8,128)} %bitcast.7, f32[1,32]{1,0:T(1,128)} %bitcast.11, f32[32,512]{1,0:T(8,128)} %up2_hbm.1, f32[32,512]{1,0:T(8,128)} %bitcast.8), custom_call_target="tpu_custom_call" | custom-call | tf_op jit(solution)/shard_map/pallas_call | solution.py:305
  27.5 0.6 %copy.9 = bf16[64,32]{0,1:T(8,128)(2,1)} copy(bf16[64,32]{0,1:T(8,128)(2,1)S(1)} %bitcast.6) | data formatting | bytes 8192

commit v8 on v7

--- a/solution.py
+++ b/solution.py
@@ -117,14 +117,17 @@
     def whole(m, c):
         return wall[m, c * NY:(c + 1) * NY].reshape(NY * cols, wall.shape[-1])
 
-    loads[0].start()
-    loads[1].start()
-    load_u.start()
-
     @pl.when(core == 1)
     def _():
         for offset in ALONG_Z[:3]:
             signal(barrier, offset, 0)
+
+    loads[0].start()
+    loads[1].start()
+    load_u.start()
+
+    @pl.when(core == 1)
+    def _():
         for offset in ALONG_Y:
             signal(barrier, offset, 1)
         for offset in ALONG_Z[3:] + ALONG_X:
@@ -249,11 +252,9 @@
         first_products()
         pl.semaphore_wait(go, 1)
         share_products(0, ALONG_Y + [HERE])
-        weight(0)
-        share(0, y, ALONG_Y + [HERE])
         pl.semaphore_wait(barrier, NZ - 1 + NX - 1)
         signal(all_in, HERE, 1)
-        for m in (1, 2):
+        for m in range(3):
             weight(m)
             share(m, y, ALONG_Y + [HERE])
         arrived(given, got_ss)

time: 28.6 us -> 28.9 us (1.010)
  the two profiles are of different devices: /device:TPU:1 before, /device:TPU:32 now
where the time goes in v8:
time: 28.9 us; the launch traced here: 28.8 us
  Pallas kernels  28.2 us (98%)
  local copies, waits for them, and re-layouts  0.6 us (2%)
    pallas_call x1, Pallas kernels, local(): pl.pallas_call(functools.partial(kernel, cols * NZ * NY), out_shape=jax.S...  28.2 us
    unnamed x1, local copies, waits for them, and re-layouts  0.6 us

profile of v8, /device:TPU:32, one launch (start us, length us, event | category | flops | bytes accessed | tf_op | source)
XLA Modules:
  0.0 28.8 jit_solution(9962914538754116726)
XLA Ops:
  0.0 28.2 %shard_map.73 = bf16[32,64]{1,0:T(8,128)(2,1)S(1)} custom-call(bf16[32,64]{1,0:T(8,128)(2,1)} %bitcast.9, f32[1,32]{1,0:T(1,128)} %bitcast.10, f32[32,512]{1,0:T(8,128)} %up1_hbm.1, f32[32,512]{1,0:T(8,128)} %bitcast.7, f32[1,32]{1,0:T(1,128)} %bitcast.11, f32[32,512]{1,0:T(8,128)} %up2_hbm.1, f32[32,512]{1,0:T(8,128)} %bitcast.8), custom_call_target="tpu_custom_call" | custom-call | tf_op jit(solution)/shard_map/pallas_call | solution.py:306
  28.2 0.6 %copy.9 = bf16[64,32]{0,1:T(8,128)(2,1)} copy(bf16[64,32]{0,1:T(8,128)(2,1)S(1)} %bitcast.6) | data formatting | bytes 8192
